TPU v7x, 512 devices: a whole 4x4x16 slice. The times are simulated.
512 devices in a mesh: ep: 128 (over z, x, core), tp: 4 (over y).
Axes of the slice: x: 4, y: 4, z: 16, core: 2. Of those that a mesh axis runs over, the one named last changes fastest.
Arguments:
- hidden: bfloat16 [512, 2048], P('ep'), may hold values from -6 to 6
- attn_gain: float32 [2048], replicated, may hold values from 0.3 to 3
- query_weight: bfloat16 [2048, 2048], P('ep', 'tp'), may hold values from -0.125 to 0.125
- head_bias: float32 [16], replicated, may hold values from -10 to -4
- key_cache: bfloat16 [512, 4, 1024, 128], P('ep', 'tp'), may hold values from -6 to 6
- value_cache: bfloat16 [512, 4, 1024, 128], P('ep', 'tp'), may hold values from -7 to 7
- lengths: int32 [512], P('ep'), may hold values from 256 to 1024, as said below
- out_weight: bfloat16 [2048, 2048], P('tp', 'ep'), may hold values from -0.125 to 0.125
- moe_gain: float32 [2048], replicated, may hold values from 0.1 to 1.9
- route_group: int32 [512], P('ep'), may hold values from 0 to 3, as said below
- route_inner: int32 [512, 2], P('ep'), may hold values from 0 to 31, as said below
- route_weight: bfloat16 [512, 2], P('ep'), may hold values from 0.25 to 1
- gate_w: bfloat16 [128, 2048, 768], P('ep', None, 'tp'), may hold values from -0.125 to 0.125
- up_w: bfloat16 [128, 2048, 768], P('ep', None, 'tp'), may hold values from -0.125 to 0.125
- down_w: bfloat16 [128, 768, 2048], P('ep', 'tp'), may hold values from -0.21875 to 0.21875
Outputs:
- mixed: bfloat16 [512, 2048], P('ep', 'tp')
Inputs may be any that keep to these rules, and one draw needn't show every extreme that they name: `lengths`: some sequence has length 1024 in every draw. Within the rows of one device (aligned blocks of 4 rows) no expert route_group * 32 + route_inner is named twice; one expert is named in every block. `route_inner`: the 2 entries of a row differ.
All inputs are finite; a program needn't handle non-finite values.
Results may differ from a plain program's by a relative error of at most 0.013.
Values may be sent and summed in bfloat16 or wider, within the bound.
A program may use at most 64 MiB of HBM per device.

v0:
```python
import jax
import jax.numpy as jnp
from jax import lax
from jax.sharding import Mesh
from jax.sharding import PartitionSpec as P

EP = ("ep_0", "ep_1", "ep_2")
rms_epsilon = 1e-06


def joined_along(tiles, dim):
    lengths = list(tiles.shape[1:])
    lengths[dim] *= tiles.shape[0]
    return jnp.moveaxis(tiles, 0, dim).reshape(lengths)


def gather_in_order(shard, axes, sequence):
    tiles = shard[None]
    for k in sequence:
        tiles = lax.all_gather(tiles, axes[k], axis=0, tiled=True)
    current = [lax.axis_size(axes[k]) for k in reversed(sequence)]
    tiles = tiles.reshape(*current, *shard.shape)
    turned = sorted(range(len(sequence)), key=lambda place: sequence[len(sequence) - 1 - place])
    return tiles.transpose(*turned, *range(len(sequence), tiles.ndim)).reshape(-1, *shard.shape)


def gathered_by_axis(shard, axes, sequence, dim):
    return joined_along(gather_in_order(shard, axes, sequence), dim)


def in_blocks(shard, dim, peers):
    lengths = shard.shape
    tiles = shard.reshape(*lengths[:dim], peers, lengths[dim] // peers, *lengths[dim + 1 :])
    return jnp.moveaxis(tiles, dim, 0)


def moved_by_axis(tiles, axes, sequence):
    lengths = [lax.axis_size(a) for a in axes]
    tiles = tiles.reshape(*lengths, *tiles.shape[1:])
    for k in sequence:
        tiles = lax.all_to_all(tiles, axes[k], split_axis=k, concat_axis=k, tiled=True)
    return tiles.reshape(-1, *tiles.shape[len(axes) :])


def core_and_chips(shard, groups, sequence, split_dim, concat_dim):
    peers = lax.axis_size(groups[0]) * lax.axis_size(groups[1])
    tiles = in_blocks(shard, split_dim, peers)
    return joined_along(moved_by_axis(tiles, groups, sequence), concat_dim)


def sum_at_owner(shard, axis, dim):
    peers = lax.axis_size(axis)
    tiles = lax.all_to_all(in_blocks(shard, dim, peers), axis, 0, 0, tiled=True)
    return jnp.sum(tiles.astype(jnp.float32), axis=0)


def rms_scale(values, gain):
    wide = values.astype(jnp.float32)
    scaled = wide * lax.rsqrt(jnp.mean(wide * wide, axis=-1, keepdims=True) + rms_epsilon)
    return (scaled * gain).astype(jnp.bfloat16)


def body(
    hidden,
    attn_gain,
    query_weight,
    head_bias,
    key_cache,
    value_cache,
    lengths,
    out_weight,
    moe_gain,
    route_group,
    route_inner,
    route_weight,
    gate_w,
    up_w,
    down_w,
):
    n_tp = lax.axis_size("tp")
    n_ep = lax.axis_size(EP)
    tokens = hidden.shape[0]
    d_model = hidden.shape[1]
    normed = rms_scale(hidden, attn_gain)
    queries = jnp.dot(
        normed, gathered_by_axis(query_weight, EP, (1, 0, 2), 0), preferred_element_type=jnp.float32
    ).astype(jnp.bfloat16)
    head_size = key_cache.shape[3]
    local_kv = key_cache.shape[1]
    cache_len = key_cache.shape[2]
    local_heads = queries.shape[1] // head_size
    group_heads = local_heads // local_kv
    queries = queries.reshape(tokens, local_kv, group_heads, head_size)
    own_bias = lax.dynamic_slice_in_dim(
        head_bias, lax.axis_index("tp") * local_heads, local_heads, 0
    )
    own_bias = own_bias.reshape(local_kv, group_heads)
    scores = jnp.einsum(
        "tkgd,tkpd->tkgp", queries, key_cache, preferred_element_type=jnp.float32
    ) * head_size ** (-0.5)
    scores = scores + own_bias[None, :, :, None]
    position = jnp.arange(cache_len, dtype=jnp.int32)
    visible = position[None, None, None, :] < lengths[:, None, None, None]
    log_keep = jnp.where(visible, jax.nn.log_sigmoid(-scores), 0.0)
    later_sum = lax.cumsum(log_keep, axis=3, reverse=True) - log_keep
    weight = jnp.where(visible, jnp.exp(jax.nn.log_sigmoid(scores) + later_sum), 0.0).astype(
        jnp.bfloat16
    )
    heads_out = jnp.einsum(
        "tkgp,tkpd->tkgd", weight, value_cache, preferred_element_type=jnp.float32
    )
    heads_out = heads_out.astype(jnp.bfloat16).reshape(tokens, -1)
    partial_value = jnp.dot(
        gathered_by_axis(heads_out, EP, (1, 0, 2), 0),
        out_weight,
        preferred_element_type=jnp.float32,
    )
    rounded = lax.optimization_barrier(partial_value.astype(jnp.bfloat16)).astype(jnp.float32)
    col_total = lax.psum(rounded.astype(jnp.bfloat16), "tp").astype(jnp.float32)
    attended = lax.all_to_all(
        col_total.astype(jnp.bfloat16), EP, split_axis=0, concat_axis=1, tiled=True
    ).astype(col_total.dtype)
    residual = (hidden.astype(jnp.float32) + attended).astype(jnp.bfloat16)
    normed_two = rms_scale(residual, moe_gain)
    per_device = gate_w.shape[0]
    experts = per_device * n_ep
    group_count = max(2, experts // 32)
    group_size = experts // group_count
    chosen = route_group[:, None] * group_size + route_inner
    matches = chosen[:, :, None] == jnp.arange(experts, dtype=jnp.int32)[None, None, :]
    picked = jnp.any(matches, axis=1).astype(jnp.bfloat16)
    mixing = jnp.sum(
        jnp.where(matches, route_weight[:, :, None].astype(jnp.float32), 0.0), axis=1
    ).astype(jnp.bfloat16)
    part_width = d_model // n_tp
    own_cols = lax.dynamic_slice_in_dim(
        normed_two, lax.axis_index("tp") * part_width, part_width, 1
    )
    outgoing = jnp.einsum("te,td->ed", picked, own_cols, preferred_element_type=jnp.float32)
    outgoing = outgoing.astype(jnp.bfloat16).reshape(n_ep, per_device, part_width)
    arrived = core_and_chips(outgoing, (("ep_0", "ep_1"), "ep_2"), (1, 0), 0, 0)
    arrived = lax.all_gather(arrived, "tp", axis=2, tiled=True)
    gated_in = jnp.einsum("sed,edf->sef", arrived, gate_w, preferred_element_type=jnp.float32)
    up_proj = jnp.einsum("sed,edf->sef", arrived, up_w, preferred_element_type=jnp.float32)
    activated = (jax.nn.silu(gated_in) * up_proj).astype(jnp.bfloat16)
    down_out = jnp.einsum("sef,efd->sed", activated, down_w, preferred_element_type=jnp.float32)
    down_rounded = lax.optimization_barrier(down_out.astype(jnp.bfloat16)).astype(jnp.float32)
    summed = sum_at_owner(down_rounded.astype(jnp.bfloat16), "tp", 2).astype(jnp.bfloat16)
    returned = lax.all_to_all(summed, EP, split_axis=0, concat_axis=0, tiled=True).reshape(
        experts, part_width
    )
    routed = jnp.dot(mixing, returned, preferred_element_type=jnp.float32)
    own_residual = lax.dynamic_slice_in_dim(
        residual, lax.axis_index("tp") * part_width, part_width, 1
    )
    return (own_residual.astype(jnp.float32) + routed).astype(jnp.bfloat16)


def solution(mesh):
    torus = Mesh(mesh.devices.reshape(16, 4, 2, mesh.shape["tp"]), ("ep_0", "ep_1", "ep_2", "tp"))
    placed = (
        P(EP, None),
        P(),
        P(EP, "tp"),
        P(),
        P(EP, "tp", None, None),
        P(EP, "tp", None, None),
        P(EP),
        P("tp", EP),
        P(),
        P(EP),
        P(EP, None),
        P(EP, None),
        P(EP, None, "tp"),
        P(EP, None, "tp"),
        P(EP, "tp", None),
    )
    return jax.shard_map(body, mesh=torus, in_specs=placed, out_specs=P(EP, "tp"), check_vma=False)
```

profile of v0, /device:TPU:1, one launch (start us, length us, event | category | flops | bytes accessed | tf_op | source)
XLA Modules:
  0.0 320.1 jit_solution(2171377821161092385)
XLA Ops:
  6.5 12.0 %all-gather = bf16[64,512]{1,0:T(8,128)(2,1)} all-gather(bf16[16,512]{1,0:T(8,128)(2,1)} %param.17), channel_id=2, replica_groups=mesh['ep_0'=16,'ep_1'=4,'ep_2'=2,'tp'=4] {'ep_1'}, dimensions={0}, use_global_device_ids=true | all-gather | bytes 81920 | tf_op jit(solution)/shard_map/all_gather | solution.py:20
  18.6 66.4 %all-gather.4.cloned.1.call-done = bf16[64,16,512]{2,1,0:T(8,128)(2,1)} async-done(((bf16[4,16,512]{2,1,0:T(8,128)(2,1)}), bf16[64,16,512]{2,1,0:T(8,128)(2,1)}) %all-gather.4.cloned.1.call-update) | async-done | bytes 1048592 | tf_op jit(solution)/shard_map/all_gather | solution.py:20
  85.0 0.7 dynamic_slice.9
  85.8 0.8 dynamic-slice
  86.5 0.8 fusion.31
  87.4 0.7 broadcast_multiply_fusion
  88.1 0.7 broadcast_add_fusion
  88.7 0.7 iota_compare_fusion
  89.5 27.5 %all-gather.6.cloned.1.call-done = bf16[128,16,512]{2,1,0:T(8,128)(2,1)} async-done(((bf16[64,16,512]{2,1,0:T(8,128)(2,1)}), bf16[128,16,512]{2,1,0:T(8,128)(2,1)}) %all-gather.6.cloned.1.call-update) | async-done | bytes 2097168 | tf_op jit(solution)/shard_map/all_gather | solution.py:20
  117.0 1.8 copy.53
  118.8 0.4 convolution_convert_fusion.4
  119.3 0.4 fusion.29
  119.7 19.8 %reduce-window.6 = f32[4,1,4,8,128]{4,3,2,1,0:T(8,128)S(1)} reduce-window(f32[4,1,4,8,128]{4,3,2,1,0:T(8,128)S(1)} %bitcast.101, f32[]{:T(128)} %constant.9.clone.1), window={size=1x1x1x1x128 pad=0_0x0_0x0_0x0_0x0_127}, to_apply=%region_1.2 | reduce-window | flops 2080768 | bytes 131076 | tf_op jit(solution)/shard_map/reduce-window
  139.5 0.1 slice_reduce_fusion
  139.7 0.7 reduce-window.9
  140.4 0.1 slice_bitcast_fusion
  140.5 0.1 broadcast.72
  140.6 0.4 convolution_convert_fusion.3
  141.0 9.1 %all_gather.24 = bf16[4,4,512]{2,1,0:T(4,128)(2,1)S(1)} all-gather(bf16[1,4,512]{2,1,0:T(4,128)(2,1)S(1)} %broadcast_in_dim_reshape.4), channel_id=1, replica_groups=mesh['ep_0'=16,'ep_1'=4,'ep_2'=2,'tp'=4] {'ep_1'}, dimensions={0}, use_global_device_ids=true | all-gather | bytes 20480 | tf_op jit(solution)/shard_map/all_gather | solution.py:20
  150.1 24.1 %all_gather.25 = bf16[64,4,512]{2,1,0:T(4,128)(2,1)S(1)} all-gather(bf16[4,4,512]{2,1,0:T(4,128)(2,1)S(1)} %all_gather.24), channel_id=1, replica_groups=mesh['ep_0'=16,'ep_1'=4,'ep_2'=2,'tp'=4] {'ep_0'}, dimensions={0}, use_global_device_ids=true | all-gather | bytes 278528 | tf_op jit(solution)/shard_map/all_gather | solution.py:20
  174.2 11.7 %all_gather.26 = bf16[128,4,512]{2,1,0:T(4,128)(2,1)S(1)} all-gather(bf16[64,4,512]{2,1,0:T(4,128)(2,1)S(1)} %all_gather.25), channel_id=1, replica_groups=mesh['ep_0'=16,'ep_1'=4,'ep_2'=2,'tp'=4] {'ep_2'}, dimensions={0}, use_global_device_ids=true | all-gather | bytes 786432 | tf_op jit(solution)/shard_map/all_gather | solution.py:20
  185.9 0.2 copy.55
  186.1 0.1 reshape_reshape.10
  186.2 0.2 convolution_convert_fusion.2
  186.5 0.1 copy.56
  186.6 15.2 %psum.7 = bf16[128,4,16]{2,1,0:T(4,128)(2,1)} all-reduce(bf16[128,4,16]{2,1,0:T(4,128)(2,1)S(1)} %bitcast.98), channel_id=1, replica_groups=mesh['ep_0'=16,'ep_1'=4,'ep_2'=2,'tp'=4] {'tp'}, use_global_device_ids=true, to_apply=%region_3.4 | all-reduce | flops 8192 | bytes 32768 | tf_op jit(solution)/shard_map/psum | solution.py:119
  201.8 15.9 %all-to-all-start = ((bf16[128,4,16]{2,1,0:T(4,128)(2,1)}), bf16[128,4,16]{2,1,0:T(4,128)(2,1)S(1)}, u32[]{:S(2)}, u32[]{:S(2)}) async-start(bf16[128,4,16]{2,1,0:T(4,128)(2,1)} %psum.7), calls=%async_computation | async-start | bytes 262144 | tf_op jit(solution)/shard_map/all_to_all | solution.py:120
  217.8 0.1 fusion.46
  217.9 15.9 %all-to-all-done = bf16[128,4,16]{2,1,0:T(4,128)(2,1)S(1)} async-done(((bf16[128,4,16]{2,1,0:T(4,128)(2,1)}), bf16[128,4,16]{2,1,0:T(4,128)(2,1)S(1)}, u32[]{:S(2)}, u32[]{:S(2)}) %all-to-all-start) | async-done | bytes 16416 | tf_op jit(solution)/shard_map/all_to_all | solution.py:120
  233.8 0.2 reshape.168
  234.0 0.1 multiply_reduce_fusion
  234.2 0.2 convolution_convert_fusion.1
  234.5 3.9 %all_to_all.33 = bf16[64,2,1,1,512]{4,0,3,2,1:T(8,128)(2,1)S(1)} all-to-all(bf16[64,2,1,1,512]{4,0,3,2,1:T(8,128)(2,1)S(1)} %copy.58), channel_id=1, replica_groups=mesh['ep_0'=16,'ep_1'=4,'ep_2'=2,'tp'=4] {'ep_2'}, dimensions={1} | all-to-all | bytes 262144 | tf_op jit(solution)/shard_map/all_to_all | solution.py:41
  238.4 0.1 copy.59
  238.5 21.2 %all_to_all.34 = bf16[64,2,1,1,512]{4,1,3,2,0:T(2,128)(2,1)S(1)} all-to-all(bf16[64,2,1,1,512]{4,1,3,2,0:T(2,128)(2,1)S(1)} %copy.59), channel_id=1, replica_groups=mesh['ep_0'=16,'ep_1'=4,'ep_2'=2,'tp'=4] {'ep_0','ep_1'}, dimensions={0} | all-to-all | bytes 262144 | tf_op jit(solution)/shard_map/all_to_all | solution.py:41
  259.8 11.2 %all_gather.27 = bf16[128,1,2048]{2,0,1:T(8,128)(2,1)S(1)} all-gather(bf16[128,1,512]{2,0,1:T(8,128)(2,1)S(1)} %reshape_reshape.11), channel_id=1, replica_groups=mesh['ep_0'=16,'ep_1'=4,'ep_2'=2,'tp'=4] {'tp'}, dimensions={2}, use_global_device_ids=true | all-gather | bytes 655360 | tf_op jit(solution)/shard_map/all_gather | solution.py:142
  271.0 0.4 convolution_bitcast_fusion.1
  271.4 2.1 fusion
  273.5 9.3 %all_to_all.35 = bf16[4,128,1,512]{3,1,2,0:T(8,128)(2,1)S(1)} all-to-all(bf16[4,128,1,512]{3,1,2,0:T(8,128)(2,1)S(1)} %bitcast.96), channel_id=1, replica_groups=mesh['ep_0'=16,'ep_1'=4,'ep_2'=2,'tp'=4] {'tp'}, dimensions={0} | all-to-all | bytes 1048576 | tf_op jit(solution)/shard_map/all_to_all | solution.py:53
  282.9 0.1 reduce_sum.44
  282.9 0.5 broadcast.80
  283.4 0.7 reduce.4
  284.1 0.7 reshape.171
  284.8 11.4 %all-to-all-start.4 = ((bf16[128,2,256]{2,1,0:T(2,128)(2,1)}), bf16[128,2,256]{2,1,0:T(2,128)(2,1)S(1)}, u32[]{:S(2)}, u32[]{:S(2)}) async-start(bf16[128,2,256]{2,1,0:T(2,128)(2,1)} %reshape.171), calls=%async_computation.4 | async-start | bytes 262144 | tf_op jit(solution)/shard_map/all_to_all | solution.py:149
  296.2 0.1 select_reduce_fusion
  296.3 16.1 %all-to-all-done.4 = bf16[128,2,256]{2,1,0:T(2,128)(2,1)S(1)} async-done(((bf16[128,2,256]{2,1,0:T(2,128)(2,1)}), bf16[128,2,256]{2,1,0:T(2,128)(2,1)S(1)}, u32[]{:S(2)}, u32[]{:S(2)}) %all-to-all-start.4) | async-done | bytes 131104 | tf_op jit(solution)/shard_map/all_to_all | solution.py:149
  312.4 0.1 reshape.172
  312.5 0.7 fusion.5
  (35 shorter events, 0.5 us)
Async XLA Ops:
  6.5 112.7 %copy-start = (bf16[4,1,1024,128]{3,2,1,0:T(8,128)(2,1)S(1)}, bf16[4,1,1024,128]{3,2,1,0:T(8,128)(2,1)}, u32[]{:S(2)}) copy-start(bf16[4,1,1024,128]{3,2,1,0:T(8,128)(2,1)} %param.19) | copy-start | bytes 3145732
  6.5 78.5 %all-gather.4.cloned.1.call-start = ((), (), s32[]{:S(2)}) async-start(), calls=%async_computation.5 | async-start | bytes 1114112 | tf_op jit(solution)/shard_map/all_gather | solution.py:20
  18.6 98.4 %all-gather.6.cloned.1.call-start = ((), (), s32[]{:S(2)}) async-start(), calls=%async_computation.6 | async-start | bytes 3145728 | tf_op jit(solution)/shard_map/all_gather | solution.py:20
  117.0 1.8 copy-start.3
  117.0 1.9 copy-start.5
  118.8 21.8 %copy-start.6 = (bf16[4,1,1024,128]{3,2,1,0:T(8,128)(2,1)S(1)}, bf16[4,1,1024,128]{3,2,1,0:T(8,128)(2,1)}, u32[]{:S(2)}) copy-start(bf16[4,1,1024,128]{3,2,1,0:T(8,128)(2,1)} %param.20) | copy-start | bytes 3145732
  140.6 45.6 %copy-start.4 = (bf16[512,16]{0,1:T(8,128)(2,1)S(1)}, bf16[512,16]{0,1:T(8,128)(2,1)}, u32[]{:S(2)}) copy-start(bf16[512,16]{0,1:T(8,128)(2,1)} %param.22) | copy-start | bytes 49156
  186.6 84.4 %copy-start.1 = (bf16[1,2048,192]{1,2,0:T(8,128)(2,1)S(1)}, bf16[1,2048,192]{1,2,0:T(8,128)(2,1)}, u32[]{:S(2)}) copy-start(bf16[1,2048,192]{1,2,0:T(8,128)(2,1)} %param.27) | copy-start | bytes 2359300
  201.8 31.9 %all-to-all-start = ((bf16[128,4,16]{2,1,0:T(4,128)(2,1)}), bf16[128,4,16]{2,1,0:T(4,128)(2,1)S(1)}, u32[]{:S(2)}, u32[]{:S(2)}) async-start(bf16[128,4,16]{2,1,0:T(4,128)(2,1)} %psum.7), calls=%async_computation | async-start | bytes 262144 | tf_op jit(solution)/shard_map/all_to_all | solution.py:120
  233.8 37.6 %copy-start.2 = (bf16[1,192,2048]{2,1,0:T(8,128)(2,1)S(1)}, bf16[1,192,2048]{2,1,0:T(8,128)(2,1)}, u32[]{:S(2)}) copy-start(bf16[1,192,2048]{2,1,0:T(8,128)(2,1)} %param.29) | copy-start | bytes 2359300
  273.5 22.8 %copy-start.7 = (bf16[4,2]{0,1:T(2,128)(2,1)S(1)}, bf16[4,2]{0,1:T(2,128)(2,1)}, u32[]{:S(2)}) copy-start(bf16[4,2]{0,1:T(2,128)(2,1)} %param.26) | copy-start | bytes 52
  284.8 27.6 %all-to-all-start.4 = ((bf16[128,2,256]{2,1,0:T(2,128)(2,1)}), bf16[128,2,256]{2,1,0:T(2,128)(2,1)S(1)}, u32[]{:S(2)}, u32[]{:S(2)}) async-start(bf16[128,2,256]{2,1,0:T(2,128)(2,1)} %reshape.171), calls=%async_computation.4 | async-start | bytes 262144 | tf_op jit(solution)/shard_map/all_to_all | solution.py:149
Sparse Core Ops, SparseCore 0:
  18.7 66.2 all-gather.3
  87.1 29.8 all-gather.5
where the time goes:
time: 321 us; the launch traced here: 320 us
  waiting for transfers between devices  126 us (39%)
  blocking collectives  118 us (37%)
  starting transfers between devices  27.4 us (9%)
  other arithmetic  24.6 us (8%)
  between operations  13.7 us (4%)
  local copies, waits for them, and re-layouts  5.95 us (2%)
  matrix products  4.82 us (2%)
    all_gather x2, waiting for transfers between devices, gather_in_order(): tiles = lax.all_gather(tiles, axes[k], axis=0, tiled=True)  93.9 us
    all_gather x4, blocking collectives, gather_in_order(): tiles = lax.all_gather(tiles, axes[k], axis=0, tiled=True)  56.9 us
    all_to_all x2, blocking collectives, moved_by_axis(): lax.all_to_all(tiles, axes[k], split_axis=k, concat_axis=k, tiled=True)  25.1 us
    another operation x2, other arithmetic  20.5 us
    all_to_all x1, waiting for transfers between devices, body(): lax.all_to_all(summed, EP, split_axis=0, concat_axis=0, tiled=True)  16.1 us
    all_to_all x1, starting transfers between devices, body(): lax.all_to_all(col_total.astype(jnp.bfloat16), EP, split_axis=0, concat_a...  15.9 us
    all_to_all x1, waiting for transfers between devices, body(): lax.all_to_all(col_total.astype(jnp.bfloat16), EP, split_axis=0, concat_a...  15.9 us
    psum x1, blocking collectives, body(): col_total = lax.psum(rounded.astype(jnp.bfloat16), 'tp').astype(jnp.float32)  15.2 us
  transfers between devices with their start and end apart: 4, of which 4 were waited for; matrix products, arithmetic and copies ran while one was open for 1% of the time, Pallas kernels for 0%

commit v1 on v0

--- a/solution.py
+++ b/solution.py
@@ -17,7 +17,9 @@
 def gather_in_order(shard, axes, sequence):
     tiles = shard[None]
     for k in sequence:
-        tiles = lax.all_gather(tiles, axes[k], axis=0, tiled=True)
+        tiles = jnp.concatenate(
+            lax.all_to_all(jnp.stack([tiles] * lax.axis_size(axes[k])), axes[k], 0, 0), axis=0
+        )
     current = [lax.axis_size(axes[k]) for k in reversed(sequence)]
     tiles = tiles.reshape(*current, *shard.shape)
     turned = sorted(range(len(sequence)), key=lambda place: sequence[len(sequence) - 1 - place])

time: 321 us -> 268 us (0.83)
  waiting for transfers between devices: 126 us -> 88.2 us
  blocking collectives: 118 us -> 98.2 us
  starting transfers between devices: 27.4 us -> 46 us
  between operations: 13.7 us -> 0.35 us
    all_gather x2 -> x0, waiting for transfers between devices: 93.9 us -> none  [gather_in_order(): tiles = lax.all_gather(tiles, axes[k], axis=0, tiled=True)]
    all_gather x4 -> x0, blocking collectives: 56.9 us -> none  [gather_in_order(): tiles = lax.all_gather(tiles, axes[k], axis=0, tiled=True)]
    all_to_all x0 -> x2, waiting for transfers between devices: none -> 56.2 us  [gather_in_order(): lax.all_to_all(jnp.stack([tiles] * lax.axis_size(axes[k])), axes[k], 0, 0)]
    all_to_all x0 -> x4, blocking collectives: none -> 37.1 us  [gather_in_order(): lax.all_to_all(jnp.stack([tiles] * lax.axis_size(axes[k])), axes[k], 0, 0)]
    all_to_all x0 -> x2, starting transfers between devices: none -> 23.1 us  [gather_in_order(): lax.all_to_all(jnp.stack([tiles] * lax.axis_size(axes[k])), axes[k], 0, 0)]
    all_to_all x1, starting transfers between devices: 15.9 us -> 11.5 us  [body(): lax.all_to_all(col_total.astype(jnp.bfloat16), EP, split_axis=0, concat_a...]
    another operation x2 -> x4, other arithmetic: 20.5 us -> 21 us
  transfers between devices with their start and end apart: 4 -> 4, of which waited for: 4 -> 4; matrix products, arithmetic and copies ran while one was open for 1% -> 0% of each run, Pallas kernels for 0% -> 0%
where the time goes in v1:
time: 268 us; the launch traced here: 267 us
  blocking collectives  98.2 us (37%)
  waiting for transfers between devices  88.2 us (33%)
  starting transfers between devices  46 us (17%)
  other arithmetic  22.3 us (8%)
  local copies, waits for them, and re-layouts  6.91 us (3%)
  matrix products  4.82 us (2%)
    all_to_all x2, waiting for transfers between devices, gather_in_order(): lax.all_to_all(jnp.stack([tiles] * lax.axis_size(axes[k])), axes[k], 0, 0)  56.2 us
    all_to_all x4, blocking collectives, gather_in_order(): lax.all_to_all(jnp.stack([tiles] * lax.axis_size(axes[k])), axes[k], 0, 0)  37.1 us
    all_to_all x2, blocking collectives, moved_by_axis(): lax.all_to_all(tiles, axes[k], split_axis=k, concat_axis=k, tiled=True)  25.1 us
    all_to_all x2, starting transfers between devices, gather_in_order(): lax.all_to_all(jnp.stack([tiles] * lax.axis_size(axes[k])), axes[k], 0, 0)  23.1 us
    another operation x2, other arithmetic  20.5 us
    all_to_all x1, waiting for transfers between devices, body(): lax.all_to_all(summed, EP, split_axis=0, concat_axis=0, tiled=True)  16.1 us
    all_to_all x1, waiting for transfers between devices, body(): lax.all_to_all(col_total.astype(jnp.bfloat16), EP, split_axis=0, concat_a...  15.9 us
    psum x1, blocking collectives, body(): col_total = lax.psum(rounded.astype(jnp.bfloat16), 'tp').astype(jnp.float32)  15.5 us
  transfers between devices with their start and end apart: 4, of which 4 were waited for; matrix products, arithmetic and copies ran while one was open for 0% of the time, Pallas kernels for 0%

profile of v1, /device:TPU:1, one launch (start us, length us, event | category | flops | bytes accessed | tf_op | source)
XLA Modules:
  0.0 266.8 jit_solution(1854134920195677448)
XLA Ops:
  0.0 0.8 stack.18
  0.8 9.1 %all_to_all.63 = bf16[4,1,16,512]{3,2,1,0:T(8,128)(2,1)S(1)} all-to-all(bf16[4,1,16,512]{3,2,1,0:T(8,128)(2,1)S(1)} %stack.18), channel_id=1, replica_groups=mesh['ep_0'=16,'ep_1'=4,'ep_2'=2,'tp'=4] {'ep_1'}, dimensions={0} | all-to-all | bytes 131072 | tf_op jit(solution)/shard_map/all_to_all | solution.py:21
  9.9 1.1 stack.19
  11.0 14.9 %all-to-all-start.1 = ((bf16[16,4,16,512]{3,2,1,0:T(8,128)(2,1)}), bf16[16,4,16,512]{3,2,1,0:T(8,128)(2,1)S(1)}, u32[]{:S(2)}, u32[]{:S(2)}) async-start(bf16[16,4,16,512]{3,2,1,0:T(8,128)(2,1)} %stack.19), calls=%async_computation.1 | async-start | bytes 2097152 | tf_op jit(solution)/shard_map/all_to_all | solution.py:21
  26.1 0.1 fusion.32
  26.3 44.3 %all-to-all-done.1 = bf16[16,4,16,512]{3,2,1,0:T(8,128)(2,1)S(1)} async-done(((bf16[16,4,16,512]{3,2,1,0:T(8,128)(2,1)}), bf16[16,4,16,512]{3,2,1,0:T(8,128)(2,1)S(1)}, u32[]{:S(2)}, u32[]{:S(2)}) %all-to-all-start.1) | async-done | bytes 1048608 | tf_op jit(solution)/shard_map/all_to_all | solution.py:21
  70.6 0.2 pad_maximum_fusion
  70.8 10.6 %all_to_all.64 = bf16[2,64,16,512]{3,2,1,0:T(8,128)(2,1)S(1)} all-to-all(bf16[2,64,16,512]{3,2,1,0:T(8,128)(2,1)S(1)} %pad_maximum_fusion), channel_id=1, replica_groups=mesh['ep_0'=16,'ep_1'=4,'ep_2'=2,'tp'=4] {'ep_2'}, dimensions={0} | all-to-all | bytes 4194304 | tf_op jit(solution)/shard_map/all_to_all | solution.py:21
  81.3 0.2 copy.46
  81.6 0.4 copy-done.5
  82.0 0.4 convolution_convert_fusion.4
  82.5 0.4 fusion.30
  82.9 19.8 %reduce-window.6 = f32[4,1,4,8,128]{4,3,2,1,0:T(8,128)S(1)} reduce-window(f32[4,1,4,8,128]{4,3,2,1,0:T(8,128)S(1)} %bitcast.113, f32[]{:T(128)} %constant.9.clone.1), window={size=1x1x1x1x128 pad=0_0x0_0x0_0x0_0x0_127}, to_apply=%region_1.2 | reduce-window | flops 2080768 | bytes 131076 | tf_op jit(solution)/shard_map/reduce-window
  102.8 0.1 slice_reduce_fusion
  102.9 0.7 reduce-window.9
  103.8 0.4 fusion.6
  104.2 6.7 %all_to_all.65 = bf16[4,1,4,512]{3,2,1,0:T(4,128)(2,1)S(1)} all-to-all(bf16[4,1,4,512]{3,2,1,0:T(4,128)(2,1)S(1)} %stack.21), channel_id=1, replica_groups=mesh['ep_0'=16,'ep_1'=4,'ep_2'=2,'tp'=4] {'ep_1'}, dimensions={0} | all-to-all | bytes 32768 | tf_op jit(solution)/shard_map/all_to_all | solution.py:21
  111.0 0.8 stack.22
  111.8 8.2 %all-to-all-start.4 = ((bf16[16,4,4,512]{3,2,1,0:T(4,128)(2,1)}), bf16[16,4,4,512]{3,2,1,0:T(4,128)(2,1)S(1)}, u32[]{:S(2)}, u32[]{:S(2)}) async-start(bf16[16,4,4,512]{3,2,1,0:T(4,128)(2,1)} %stack.22), calls=%async_computation.4 | async-start | bytes 524288 | tf_op jit(solution)/shard_map/all_to_all | solution.py:21
  120.0 0.8 dynamic-slice
  120.8 11.9 %all-to-all-done.4 = bf16[16,4,4,512]{3,2,1,0:T(4,128)(2,1)S(1)} async-done(((bf16[16,4,4,512]{3,2,1,0:T(4,128)(2,1)}), bf16[16,4,4,512]{3,2,1,0:T(4,128)(2,1)S(1)}, u32[]{:S(2)}, u32[]{:S(2)}) %all-to-all-start.4) | async-done | bytes 262176 | tf_op jit(solution)/shard_map/all_to_all | solution.py:21
  132.7 0.2 pad_maximum_fusion.1
  133.0 10.7 %all_to_all.66 = bf16[2,64,4,512]{3,2,1,0:T(4,128)(2,1)S(1)} all-to-all(bf16[2,64,4,512]{3,2,1,0:T(4,128)(2,1)S(1)} %pad_maximum_fusion.1), channel_id=1, replica_groups=mesh['ep_0'=16,'ep_1'=4,'ep_2'=2,'tp'=4] {'ep_2'}, dimensions={0} | all-to-all | bytes 1048576 | tf_op jit(solution)/shard_map/all_to_all | solution.py:21
  143.6 0.2 copy.66
  143.8 0.1 reshape_reshape.18
  144.0 0.2 convolution_convert_fusion.2
  144.2 0.1 copy.49
  144.4 15.5 %psum.7 = bf16[128,4,16]{2,1,0:T(4,128)(2,1)} all-reduce(bf16[128,4,16]{2,1,0:T(4,128)(2,1)S(1)} %bitcast.110), channel_id=1, replica_groups=mesh['ep_0'=16,'ep_1'=4,'ep_2'=2,'tp'=4] {'tp'}, use_global_device_ids=true, to_apply=%region_3.4 | all-reduce | flops 8192 | bytes 32768 | tf_op jit(solution)/shard_map/psum | solution.py:121
  159.9 11.5 %all-to-all-start.6 = ((bf16[128,4,16]{2,1,0:T(4,128)(2,1)}), bf16[128,4,16]{2,1,0:T(4,128)(2,1)S(1)}, u32[]{:S(2)}, u32[]{:S(2)}) async-start(bf16[128,4,16]{2,1,0:T(4,128)(2,1)} %psum.7), calls=%async_computation.6 | async-start | bytes 262144 | tf_op jit(solution)/shard_map/all_to_all | solution.py:122
  171.3 0.1 fusion.47
  171.4 15.9 %all-to-all-done.6 = bf16[128,4,16]{2,1,0:T(4,128)(2,1)S(1)} async-done(((bf16[128,4,16]{2,1,0:T(4,128)(2,1)}), bf16[128,4,16]{2,1,0:T(4,128)(2,1)S(1)}, u32[]{:S(2)}, u32[]{:S(2)}) %all-to-all-start.6) | async-done | bytes 16416 | tf_op jit(solution)/shard_map/all_to_all | solution.py:122
  187.4 0.2 reshape.170
  187.5 0.1 multiply_reduce_fusion
  187.7 0.2 convolution_convert_fusion.1
  188.0 3.9 %all_to_all.67 = bf16[64,2,1,1,512]{4,0,3,2,1:T(8,128)(2,1)S(1)} all-to-all(bf16[64,2,1,1,512]{4,0,3,2,1:T(8,128)(2,1)S(1)} %copy.51), channel_id=1, replica_groups=mesh['ep_0'=16,'ep_1'=4,'ep_2'=2,'tp'=4] {'ep_2'}, dimensions={1} | all-to-all | bytes 262144 | tf_op jit(solution)/shard_map/all_to_all | solution.py:43
  191.9 0.1 copy.52
  192.1 21.2 %all_to_all.68 = bf16[64,2,1,1,512]{4,1,3,2,0:T(2,128)(2,1)S(1)} all-to-all(bf16[64,2,1,1,512]{4,1,3,2,0:T(2,128)(2,1)S(1)} %copy.52), channel_id=1, replica_groups=mesh['ep_0'=16,'ep_1'=4,'ep_2'=2,'tp'=4] {'ep_0','ep_1'}, dimensions={0} | all-to-all | bytes 262144 | tf_op jit(solution)/shard_map/all_to_all | solution.py:43
  213.3 11.2 %all_gather.3 = bf16[128,1,2048]{2,0,1:T(8,128)(2,1)S(1)} all-gather(bf16[128,1,512]{2,0,1:T(8,128)(2,1)S(1)} %reshape_reshape.19), channel_id=1, replica_groups=mesh['ep_0'=16,'ep_1'=4,'ep_2'=2,'tp'=4] {'tp'}, dimensions={2}, use_global_device_ids=true | all-gather | bytes 655360 | tf_op jit(solution)/shard_map/all_gather | solution.py:144
  224.6 0.4 convolution_bitcast_fusion.1
  224.9 2.1 fusion
  227.1 9.3 %all_to_all.69 = bf16[4,128,1,512]{3,1,2,0:T(8,128)(2,1)S(1)} all-to-all(bf16[4,128,1,512]{3,1,2,0:T(8,128)(2,1)S(1)} %bitcast.107), channel_id=1, replica_groups=mesh['ep_0'=16,'ep_1'=4,'ep_2'=2,'tp'=4] {'tp'}, dimensions={0} | all-to-all | bytes 1048576 | tf_op jit(solution)/shard_map/all_to_all | solution.py:55
  236.5 0.5 broadcast.86
  237.0 0.7 reduce.4
  237.7 0.7 reshape.172
  238.4 11.4 %all-to-all-start.10 = ((bf16[128,2,256]{2,1,0:T(2,128)(2,1)}), bf16[128,2,256]{2,1,0:T(2,128)(2,1)S(1)}, u32[]{:S(2)}, u32[]{:S(2)}) async-start(bf16[128,2,256]{2,1,0:T(2,128)(2,1)} %reshape.172), calls=%async_computation.10 | async-start | bytes 262144 | tf_op jit(solution)/shard_map/all_to_all | solution.py:151
  249.9 16.1 %all-to-all-done.10 = bf16[128,2,256]{2,1,0:T(2,128)(2,1)S(1)} async-done(((bf16[128,2,256]{2,1,0:T(2,128)(2,1)}), bf16[128,2,256]{2,1,0:T(2,128)(2,1)S(1)}, u32[]{:S(2)}, u32[]{:S(2)}) %all-to-all-start.10) | async-done | bytes 131104 | tf_op jit(solution)/shard_map/all_to_all | solution.py:151
  265.9 0.1 reshape.173
  266.0 0.7 fusion.5
  (47 shorter events, 0.9 us)
Async XLA Ops:
  0.0 82.5 %copy-start = (bf16[4,1,1024,128]{3,2,1,0:T(8,128)(2,1)S(1)}, bf16[4,1,1024,128]{3,2,1,0:T(8,128)(2,1)}, u32[]{:S(2)}) copy-start(bf16[4,1,1024,128]{3,2,1,0:T(8,128)(2,1)} %param.19) | copy-start | bytes 3145732
  0.0 26.0 %copy-start.9 = (f32[16]{0:T(128)S(1)}, f32[16]{0:T(128)}, u32[]{:S(2)}) copy-start(f32[16]{0:T(128)} %param.18) | copy-start | bytes 196
  0.0 26.1 %copy-start.3 = (bf16[4,2048]{1,0:T(4,128)(2,1)S(1)}, bf16[4,2048]{1,0:T(4,128)(2,1)}, u32[]{:S(2)}) copy-start(bf16[4,2048]{1,0:T(4,128)(2,1)} %param.15) | copy-start | bytes 49156
  0.0 26.2 %copy-start.7 = (s32[4]{0:T(128)S(1)}, s32[4]{0:T(128)}, u32[]{:S(2)}) copy-start(s32[4]{0:T(128)} %param.21) | copy-start | bytes 52
  11.0 59.5 %all-to-all-start.1 = ((bf16[16,4,16,512]{3,2,1,0:T(8,128)(2,1)}), bf16[16,4,16,512]{3,2,1,0:T(8,128)(2,1)S(1)}, u32[]{:S(2)}, u32[]{:S(2)}) async-start(bf16[16,4,16,512]{3,2,1,0:T(8,128)(2,1)} %stack.19), calls=%async_computation.1 | async-start | bytes 2097152 | tf_op jit(solution)/shard_map/all_to_all | solution.py:21
  81.3 0.7 copy-start.5
  81.6 22.2 %copy-start.8 = (bf16[4,1,1024,128]{3,2,1,0:T(8,128)(2,1)S(1)}, bf16[4,1,1024,128]{3,2,1,0:T(8,128)(2,1)}, u32[]{:S(2)}) copy-start(bf16[4,1,1024,128]{3,2,1,0:T(8,128)(2,1)} %param.20) | copy-start | bytes 3145732
  82.5 38.3 %copy-start.10 = (s32[4]{0:T(128)S(1)}, s32[4]{0:T(128)}, u32[]{:S(2)}) copy-start(s32[4]{0:T(128)} %param.24) | copy-start | bytes 52
  82.5 38.3 %copy-start.6 = (s32[4,2]{0,1:T(2,128)S(1)}, s32[4,2]{0,1:T(2,128)}, u32[]{:S(2)}) copy-start(s32[4,2]{0,1:T(2,128)} %param.25) | copy-start | bytes 100
  111.8 20.9 %all-to-all-start.4 = ((bf16[16,4,4,512]{3,2,1,0:T(4,128)(2,1)}), bf16[16,4,4,512]{3,2,1,0:T(4,128)(2,1)S(1)}, u32[]{:S(2)}, u32[]{:S(2)}) async-start(bf16[16,4,4,512]{3,2,1,0:T(4,128)(2,1)} %stack.22), calls=%async_computation.4 | async-start | bytes 524288 | tf_op jit(solution)/shard_map/all_to_all | solution.py:21
  120.0 24.0 %copy-start.4 = (bf16[512,16]{0,1:T(8,128)(2,1)S(1)}, bf16[512,16]{0,1:T(8,128)(2,1)}, u32[]{:S(2)}) copy-start(bf16[512,16]{0,1:T(8,128)(2,1)} %param.22) | copy-start | bytes 49156
  144.4 80.2 %copy-start.1 = (bf16[1,2048,192]{1,2,0:T(8,128)(2,1)S(1)}, bf16[1,2048,192]{1,2,0:T(8,128)(2,1)}, u32[]{:S(2)}) copy-start(bf16[1,2048,192]{1,2,0:T(8,128)(2,1)} %param.27) | copy-start | bytes 2359300
  159.9 27.5 %all-to-all-start.6 = ((bf16[128,4,16]{2,1,0:T(4,128)(2,1)}), bf16[128,4,16]{2,1,0:T(4,128)(2,1)S(1)}, u32[]{:S(2)}, u32[]{:S(2)}) async-start(bf16[128,4,16]{2,1,0:T(4,128)(2,1)} %psum.7), calls=%async_computation.6 | async-start | bytes 262144 | tf_op jit(solution)/shard_map/all_to_all | solution.py:122
  187.4 37.6 %copy-start.2 = (bf16[1,192,2048]{2,1,0:T(8,128)(2,1)S(1)}, bf16[1,192,2048]{2,1,0:T(8,128)(2,1)}, u32[]{:S(2)}) copy-start(bf16[1,192,2048]{2,1,0:T(8,128)(2,1)} %param.29) | copy-start | bytes 2359300
  227.0 22.8 %copy-start.11 = (bf16[4,2]{0,1:T(2,128)(2,1)S(1)}, bf16[4,2]{0,1:T(2,128)(2,1)}, u32[]{:S(2)}) copy-start(bf16[4,2]{0,1:T(2,128)(2,1)} %param.26) | copy-start | bytes 52
  238.4 27.6 %all-to-all-start.10 = ((bf16[128,2,256]{2,1,0:T(2,128)(2,1)}), bf16[128,2,256]{2,1,0:T(2,128)(2,1)S(1)}, u32[]{:S(2)}, u32[]{:S(2)}) async-start(bf16[128,2,256]{2,1,0:T(2,128)(2,1)} %reshape.172), calls=%async_computation.10 | async-start | bytes 262144 | tf_op jit(solution)/shard_map/all_to_all | solution.py:151
